TPU v7x, 128 devices: a whole 4x4x4 slice. The times are simulated.
128 devices in a mesh: fs: 16 (over z, x), tp: 8 (over y, core).
Axes of the slice: x: 4, y: 4, z: 4, core: 2. Of those that a mesh axis runs over, the one named last changes fastest.
Arguments:
- h_saved: bfloat16 [32768, 2048], P('fs'), may hold values from -6 to 6
- conv_cotan: bfloat16 [32768, 2560], P('fs', 'tp'), may hold values from -64 to 64
- lru_out: bfloat16 [32768, 2560], P('fs', 'tp'), may hold values from -64 to 64
- out_cotan: bfloat16 [32768, 2048], P('fs'), may hold values from -6 to 6
- basis_in: bfloat16 [2048, 256], P('fs'), may hold values from -1.41421356 to 1.41421356
- basis_out: bfloat16 [2048, 256], P('fs'), may hold values from -1.41421356 to 1.41421356
- weight_in: float32 [2048, 2560], P('fs', 'tp'), may hold values from -0.125 to 0.125
- weight_out: float32 [2560, 2048], P('tp', 'fs'), may hold values from -0.125 to 0.125
- first_in: float32 [256, 2560], P('fs', 'tp'), may hold values from -6 to 6
- second_in: float32 [256, 2560], P('fs', 'tp'), may hold values from 0.05 to 2
- first_out: float32 [256, 2560], P('fs', 'tp'), may hold values from -6 to 6
- second_out: float32 [256, 2560], P('fs', 'tp'), may hold values from 0.05 to 2
Outputs:
- step_in: float32 [2048, 2560], P('fs', 'tp')
- new_weight_in: float32 [2048, 2560], P('fs', 'tp')
- copy_in: bfloat16 [2048, 2560], P(None, 'tp')
- new_first_in: float32 [256, 2560], P('fs', 'tp')
- new_second_in: float32 [256, 2560], P('fs', 'tp')
- step_out: float32 [2560, 2048], P('tp', 'fs')
- new_weight_out: float32 [2560, 2048], P('tp', 'fs')
- copy_out: bfloat16 [2560, 2048], P('tp')
- new_first_out: float32 [256, 2560], P('fs', 'tp')
- new_second_out: float32 [256, 2560], P('fs', 'tp')
All inputs are finite; a program needn't handle non-finite values.
Results may differ from a plain program's by a relative error of at most 0.0046.
Values may be sent and summed in bfloat16 or wider, within the bound.
No kernel may reach another device: no remote copies, remote signals or barrier semaphores. Data moves between devices by JAX's collectives and lax.ppermute only.
A program may use at most 128 MiB of HBM per device.

v0:
```python
import math
import jax
import jax.numpy as jnp
from jax import lax
from jax.sharding import Mesh
from jax.sharding import PartitionSpec as P

D_RNN = 2560
RANK = 256
FS = ("fs_0", "fs_1")
FS_TP = ("fs_0", "fs_1", "tp_0", "tp_1")
TP = ("tp_0", "tp_1")


def laid_out(blocks, dim):
    blocks = jnp.moveaxis(blocks, 0, dim)
    lengths = blocks.shape
    return blocks.reshape(*lengths[:dim], lengths[dim] * lengths[dim + 1], *lengths[dim + 2 :])


def sent_to_all(array, axis):
    copies = jnp.broadcast_to(array, (lax.axis_size(axis), *array.shape))
    return lax.all_to_all(copies, axis, split_axis=0, concat_axis=0, tiled=True)


def gather_directly(array, axis, dim):
    return laid_out(sent_to_all(array, axis), dim)


def in_one_piece(arrays, axis, dim, along):
    ends, at = ([], 0)
    for a in arrays[:-1]:
        at += a.shape[along]
        ends.append(at)
    both = jnp.concatenate(arrays, axis=along)
    return tuple(jnp.split(gather_directly(both, axis, dim), ends, axis=along))


def split_up(array, dim, size):
    lengths = array.shape
    blocks = array.reshape(*lengths[:dim], size, lengths[dim] // size, *lengths[dim + 1 :])
    return jnp.moveaxis(blocks, dim, 0)


def sent_and_summed(array, axis, dim):
    blocks = split_up(array, dim, lax.axis_size(axis))
    arrived = lax.all_to_all(blocks, axis, split_axis=0, concat_axis=0, tiled=True)
    return arrived.sum(axis=0)


def sent_together(arrays, axis, dim, along):
    both = jnp.concatenate(arrays, axis=along)
    filled, at, done = (sent_and_summed(both, axis, dim), 0, [])
    for a in arrays:
        done.append(lax.slice_in_dim(filled, at, at + a.shape[along], axis=along))
        at += a.shape[along]
    return tuple(done)


def by_axis(array, axes):
    for axis in axes:
        array = lax.psum(array, axis)
    return array


def in_one_piece_2(arrays, axis, dim, along):
    widths = [a.shape[along] for a in arrays]
    both = jnp.concatenate(arrays, axis=along)
    filled = lax.all_gather(both, axis, axis=dim, tiled=True)
    return tuple(jnp.split(filled, [sum(widths[:k]) for k in range(1, len(widths))], axis=along))


def turned_gather(arrays, axis, dims):
    turned = [jnp.moveaxis(a, dim, 0) for a, dim in zip(arrays, dims)]
    widths = [t[0].size for t in turned]
    both = jnp.concatenate([t.reshape(-1, w) for t, w in zip(turned, widths)], axis=1)
    filled = lax.all_gather(both, axis, axis=0, tiled=True)
    blocks = jnp.split(filled, [sum(widths[:k]) for k in range(1, len(widths))], axis=1)
    return tuple(
        (
            jnp.moveaxis(b.reshape(-1, *t.shape[1:]), 0, dim)
            for b, t, dim in zip(blocks, turned, dims)
        )
    )


def split_product(narrow, wide):
    upper = lax.optimization_barrier(wide.astype(jnp.bfloat16))
    lower = (wide - upper.astype(jnp.float32)).astype(jnp.bfloat16)
    turned = jnp.transpose(narrow)
    first_part = jnp.dot(turned, upper, preferred_element_type=jnp.float32)
    second_part = jnp.dot(turned, lower, preferred_element_type=jnp.float32)
    return first_part + second_part


def moments(proj, factor, first, second):
    scaled = factor * proj
    first_new = 0.8 * first + 0.2 * scaled
    second_new = 0.9 * second + 0.1 * scaled * scaled
    direction = (first_new / (jnp.sqrt(second_new) + 1e-08)).astype(jnp.bfloat16)
    return (first_new, second_new, direction)


def shards(
    h_saved,
    conv_cotan,
    lru_out,
    out_cotan,
    basis_in,
    basis_out,
    weight_in,
    weight_out,
    first_in,
    second_in,
    first_out,
    second_out,
):
    pairs = ((h_saved, conv_cotan), (out_cotan, lru_out))
    partial_value = []
    wholes = in_one_piece((basis_in, basis_out), FS, 0, 1)
    for number in range(2):
        reduced = jnp.dot(pairs[number][0], wholes[number], preferred_element_type=jnp.float32)
        partial_value.append(split_product(pairs[number][1], reduced).T)
    proj_in, proj_out = sent_together((partial_value[0], partial_value[1]), FS, 0, 1)
    total = by_axis(jnp.sum(proj_in * proj_in) + jnp.sum(proj_out * proj_out), FS_TP)
    factor = math.sqrt(2.0 * RANK * D_RNN) * lax.rsqrt(total + 1e-06)
    first_a, second_a, dir_in = moments(proj_in, factor, first_in, second_in)
    first_b, second_b, dir_out = moments(proj_out, factor, first_out, second_out)
    full_in, full_out = in_one_piece_2((dir_in, dir_out), FS, 0, 1)
    step_in = jnp.dot(basis_in, full_in, preferred_element_type=jnp.float32)
    step_out = jnp.dot(basis_out, full_out, preferred_element_type=jnp.float32).T
    new_in = weight_in - 0.02 * step_in
    new_out = weight_out - 0.02 * step_out
    copy_in, copy_out = turned_gather(
        (new_in.astype(jnp.bfloat16), new_out.astype(jnp.bfloat16)), FS, (0, 1)
    )
    return (
        step_in,
        new_in,
        copy_in,
        first_a,
        second_a,
        step_out,
        new_out,
        copy_out,
        first_b,
        second_b,
    )


def solution(mesh):
    finer = Mesh(mesh.devices.reshape(4, 4, 4, 2), ("fs_0", "fs_1", "tp_0", "tp_1"))
    placed = (
        P(FS, None),
        P(FS, TP),
        P(FS, TP),
        P(FS, None),
        P(FS, None),
        P(FS, None),
        P(FS, TP),
        P(TP, FS),
        P(FS, TP),
        P(FS, TP),
        P(FS, TP),
        P(FS, TP),
    )
    return jax.shard_map(
        shards,
        mesh=finer,
        in_specs=placed,
        out_specs=(
            P(FS, TP),
            P(FS, TP),
            P(None, TP),
            P(FS, TP),
            P(FS, TP),
            P(TP, FS),
            P(TP, FS),
            P(TP, None),
            P(FS, TP),
            P(FS, TP),
        ),
        check_vma=False,
    )
```

profile of v0, /device:TPU:0, one launch (start us, length us, event | category | flops | bytes accessed | tf_op | source)
XLA Modules:
  0.0 189.7 jit_solution(8411399123699626168)
XLA Ops:
  7.2 1.0 pad_maximum_fusion.2
  8.4 36.4 %all_to_all.10 = bf16[16,128,512]{2,1,0:T(8,128)(2,1)S(1)} all-to-all(bf16[16,128,512]{2,1,0:T(8,128)(2,1)S(1)} %broadcast_in_dim.3), channel_id=1, replica_groups=mesh['fs_0'=4,'fs_1'=4,'tp_0'=4,'tp_1'=2] {'fs_0','fs_1'}, dimensions={0} | all-to-all | bytes 4194304 | tf_op jit(solution)/shard_map/all_to_all | solution.py:23
  44.9 5.9 %fusion.10 = (bf16[2048,256]{0,1:T(8,128)(2,1)S(1)}, f32[2048,256]{0,1:T(8,128)S(1)}) fusion(bf16[2048,2048]{1,0:T(8,128)(2,1)} %param.15, bf16[2048,512]{1,0:T(8,128)(2,1)S(1)} %bitcast.23), kind=kOutput, calls=%fused_computation.33 | convolution fusion | flops 2148007936 | bytes 12582912 | tf_op jit(solution)/shard_map/dot_general | solution.py:122
  50.8 2.4 %fusion.11 = (bf16[2048,256]{0,1:T(8,128)(2,1)S(1)}, f32[2048,256]{0,1:T(8,128)S(1)}) fusion(bf16[2048,2048]{1,0:T(8,128)(2,1)S(1)} %bitcast.26, bf16[2048,512]{1,0:T(8,128)(2,1)S(1)} %bitcast.24), kind=kOutput, calls=%fused_computation.34 | convolution fusion | flops 2148007936 | bytes 12582912 | tf_op jit(solution)/shard_map/dot_general | solution.py:122
  53.2 0.5 fusion.13
  53.8 0.6 convolution_add_fusion
  54.4 0.7 copy-done.1
  55.1 0.5 fusion.12
  55.6 0.6 convolution_add_fusion.1
  56.4 0.2 copy.22
  56.6 15.2 %all_to_all.11 = f32[16,16,640]{2,1,0:T(8,128)S(1)} all-to-all(f32[16,16,640]{2,1,0:T(8,128)S(1)} %bitcast.22), channel_id=1, replica_groups=mesh['fs_0'=4,'fs_1'=4,'tp_0'=4,'tp_1'=2] {'fs_0','fs_1'}, dimensions={0} | all-to-all | bytes 1310720 | tf_op jit(solution)/shard_map/all_to_all | solution.py:47
  71.9 0.7 multiply_reduce_fusion
  73.9 9.1 %psum.28 = f32[]{:T(128)} all-reduce(f32[]{:T(128)S(6)} %add.42), channel_id=1, replica_groups=mesh['fs_0'=4,'fs_1'=4,'tp_0'=4,'tp_1'=2] {'fs_0'}, use_global_device_ids=true, to_apply=%region_3.0 | all-reduce | flops 1 | bytes 8 | tf_op jit(solution)/shard_map/psum | solution.py:62
  83.0 9.6 %psum.29 = f32[]{:T(128)} all-reduce(f32[]{:T(128)} %psum.28), channel_id=1, replica_groups=mesh['fs_0'=4,'fs_1'=4,'tp_0'=4,'tp_1'=2] {'fs_1'}, use_global_device_ids=true, to_apply=%region_4.0 | all-reduce | flops 1 | bytes 8 | tf_op jit(solution)/shard_map/psum | solution.py:62
  92.6 11.4 %psum.30 = f32[]{:T(128)} all-reduce(f32[]{:T(128)} %psum.29), channel_id=1, replica_groups=mesh['fs_0'=4,'fs_1'=4,'tp_0'=4,'tp_1'=2] {'tp_0'}, use_global_device_ids=true, to_apply=%region_5.0 | all-reduce | flops 1 | bytes 8 | tf_op jit(solution)/shard_map/psum | solution.py:62
  103.9 3.1 %psum.31 = f32[]{:T(128)} all-reduce(f32[]{:T(128)} %psum.30), channel_id=1, replica_groups=mesh['fs_0'=4,'fs_1'=4,'tp_0'=4,'tp_1'=2] {'tp_1'}, use_global_device_ids=true, to_apply=%region_6.0 | all-reduce | flops 1 | bytes 8 | tf_op jit(solution)/shard_map/psum | solution.py:62
  107.8 0.7 divide_convert_fusion.1
  108.5 21.7 %all_gather.6 = bf16[256,640]{1,0:T(8,128)(2,1)S(1)} all-gather(bf16[16,640]{1,0:T(8,128)(2,1)S(1)} %pad_maximum_fusion.3), channel_id=1, replica_groups=mesh['fs_0'=4,'fs_1'=4,'tp_0'=4,'tp_1'=2] {'fs_0','fs_1'}, dimensions={0}, use_global_device_ids=true | all-gather | bytes 348160 | tf_op jit(solution)/shard_map/all_gather | solution.py:69
  130.2 0.3 fusion.2
  130.6 1.0 fusion.7
  131.5 0.7 convert_bitcast_fusion
  132.2 0.7 pad_maximum_fusion.1
  132.9 46.4 %all-gather.2.cloned.1.call-done = bf16[2048,640]{0,1:T(8,128)(2,1)} async-done(((bf16[128,640]{0,1:T(8,128)(2,1)}), bf16[2048,640]{0,1:T(8,128)(2,1)}) %all-gather.2.cloned.1.call-update) | async-done | bytes 2621456 | tf_op jit(solution)/shard_map/all_gather | solution.py:77
  179.4 3.5 %slice_bitcast_fusion = (bf16[320,2048]{1,0:T(8,128)(2,1)}, bf16[2048,320]{0,1:T(8,128)(2,1)}) fusion(bf16[2048,640]{0,1:T(8,128)(2,1)} %all-gather.2.cloned.1.call-done), kind=kLoop, calls=%fused_computation.4 | loop fusion | bytes 5242880 | tf_op jit(solution)/shard_map/transpose | solution.py:81
  (32 shorter events, 0.5 us)
Async XLA Ops:
  7.2 46.1 %copy-start = (bf16[2048,320]{0,1:T(8,128)(2,1)S(1)}, bf16[2048,320]{0,1:T(8,128)(2,1)}, u32[]{:S(2)}) copy-start(bf16[2048,320]{0,1:T(8,128)(2,1)} %param.14) | copy-start | bytes 3932164
  7.2 172.2 %all-gather.2.cloned.1.call-start = ((), (), s32[]{:S(2)}) async-start(), calls=%async_computation.2 | async-start | bytes 2785280 | tf_op jit(solution)/shard_map/all_gather | solution.py:77
  8.4 42.4 %slice-start = ((s8[8388608]{0:T(1024)(128)(4,1)}), s8[4194304]{0:T(1024)(128)(4,1)S(1)}, s32[]{:S(2)}) async-start(s8[8388608]{0:T(1024)(128)(4,1)} %bitcast.25), calls=%async_computation.3 | async-start | bytes 8388608
  44.9 5.9 %slice-start.1 = ((s8[8388608]{0:T(1024)(128)(4,1)}), s8[4194304]{0:T(1024)(128)(4,1)S(1)}, s32[]{:S(2)}) async-start(s8[8388608]{0:T(1024)(128)(4,1)} %bitcast.25), calls=%async_computation.4 | async-start | bytes 8388608
  53.8 1.3 copy-start.1
  56.2 51.5 %copy-start.7 = (f32[16,320]{1,0:T(8,128)S(1)}, f32[16,320]{1,0:T(8,128)}, u32[]{:S(2)}) copy-start(f32[16,320]{1,0:T(8,128)} %param.21) | copy-start | bytes 61444
  56.2 51.5 %copy-start.8 = (f32[16,320]{1,0:T(8,128)S(1)}, f32[16,320]{1,0:T(8,128)}, u32[]{:S(2)}) copy-start(f32[16,320]{1,0:T(8,128)} %param.20) | copy-start | bytes 61444
  56.3 51.5 %copy-start.9 = (f32[16,320]{1,0:T(8,128)S(1)}, f32[16,320]{1,0:T(8,128)}, u32[]{:S(2)}) copy-start(f32[16,320]{1,0:T(8,128)} %param.23) | copy-start | bytes 61444
  56.3 51.5 %copy-start.10 = (f32[16,320]{1,0:T(8,128)S(1)}, f32[16,320]{1,0:T(8,128)}, u32[]{:S(2)}) copy-start(f32[16,320]{1,0:T(8,128)} %param.22) | copy-start | bytes 61444
  56.3 73.9 %copy-start.4 = (bf16[128,256]{1,0:T(8,128)(2,1)S(1)}, bf16[128,256]{1,0:T(8,128)(2,1)}, u32[]{:S(2)}) copy-start(bf16[128,256]{1,0:T(8,128)(2,1)} %param.17) | copy-start | bytes 196612
  56.3 74.2 %copy-start.3 = (bf16[128,256]{1,0:T(8,128)(2,1)S(1)}, bf16[128,256]{1,0:T(8,128)(2,1)}, u32[]{:S(2)}) copy-start(bf16[128,256]{1,0:T(8,128)(2,1)} %param.16) | copy-start | bytes 196612
  56.4 74.2 %copy-start.5 = (f32[128,320]{0,1:T(8,128)S(1)}, f32[128,320]{0,1:T(8,128)}, u32[]{:S(2)}) copy-start(f32[128,320]{0,1:T(8,128)} %param.18) | copy-start | bytes 491524
  56.6 74.9 %copy-start.6 = (f32[320,128]{1,0:T(8,128)S(1)}, f32[320,128]{1,0:T(8,128)}, u32[]{:S(2)}) copy-start(f32[320,128]{1,0:T(8,128)} %param.19) | copy-start | bytes 491524
  130.5 52.4 %copy-start.2 = (f32[320,128]{1,0:T(8,128)}, f32[320,128]{1,0:T(8,128)S(1)}, u32[]{:S(2)}) copy-start(f32[320,128]{1,0:T(8,128)S(1)} %fusion.2) | copy-start | bytes 491524
Sparse Core Ops, SparseCore 0:
  133.0 46.2 all-gather.1
where the time goes:
time: 190 us
  blocking collectives  106 us (56%)
  waiting for transfers between devices  46.5 us (24%)
  between operations  16.3 us (9%)
  matrix products  11.8 us (6%)
  local copies, waits for them, and re-layouts  4.78 us (3%)
  other arithmetic  3.89 us (2%)
    all_gather x1, waiting for transfers between devices, turned_gather(): filled = lax.all_gather(both, axis, axis=0, tiled=True)  46.4 us
    all_to_all x1, blocking collectives, sent_to_all(): return lax.all_to_all(copies, axis, split_axis=0, concat_axis=0, tiled=True)  36.4 us
    psum x4, blocking collectives, by_axis(): array = lax.psum(array, axis)  33.1 us
    all_gather x1, blocking collectives, in_one_piece_2(): filled = lax.all_gather(both, axis, axis=dim, tiled=True)  21.7 us
    all_to_all x1, blocking collectives, sent_and_summed(): lax.all_to_all(blocks, axis, split_axis=0, concat_axis=0, tiled=True)  15.2 us
    dot_general x2, matrix products, shards(): jnp.dot(pairs[number][0], wholes[number], preferred_element_type=jnp.floa...  8.31 us
  transfers between devices with their start and end apart: 1, of which 1 were waited for; matrix products, arithmetic and copies ran while one was open for 0% of the time, Pallas kernels for 0%

commit v1 on v0

--- a/solution.py
+++ b/solution.py
@@ -74,7 +74,10 @@
     turned = [jnp.moveaxis(a, dim, 0) for a, dim in zip(arrays, dims)]
     widths = [t[0].size for t in turned]
     both = jnp.concatenate([t.reshape(-1, w) for t, w in zip(turned, widths)], axis=1)
-    filled = lax.all_gather(both, axis, axis=0, tiled=True)
+    count = lax.axis_size(axis)
+    pieces = jnp.stack([both for _ in range(count)])
+    pieces = lax.all_to_all(pieces, axis, split_axis=0, concat_axis=0)
+    filled = jnp.concatenate(pieces, axis=0)
     blocks = jnp.split(filled, [sum(widths[:k]) for k in range(1, len(widths))], axis=1)
     return tuple(
         (

time: 190 us -> 173 us (0.911)
  waiting for transfers between devices: 46.5 us -> 0 us
  blocking collectives: 106 us -> 140 us
  between operations: 16.3 us -> 2.92 us
  local copies, waits for them, and re-layouts: 4.78 us -> 14.1 us
    all_gather x1 -> x0, waiting for transfers between devices: 46.4 us -> none  [turned_gather(): filled = lax.all_gather(both, axis, axis=0, tiled=True)]
    all_to_all x0 -> x1, blocking collectives: none -> 33.9 us  [turned_gather(): pieces = lax.all_to_all(pieces, axis, split_axis=0, concat_axis=0)]
    all_to_all x0 -> x1, local copies, waits for them, and re-layouts: none -> 4.38 us  [turned_gather(): pieces = lax.all_to_all(pieces, axis, split_axis=0, concat_axis=0)]
    unnamed x26 -> x28, local copies, waits for them, and re-layouts: 0.83 us -> 4.87 us
  transfers between devices with their start and end apart: 1 -> 0, of which waited for: 1 -> 0; matrix products, arithmetic and copies ran while one was open for 0% -> 0% of each run, Pallas kernels for 0% -> 0%
where the time goes in v1:
time: 173 us; the launch traced here: 172 us
  blocking collectives  140 us (81%)
  local copies, waits for them, and re-layouts  14.1 us (8%)
  matrix products  11.8 us (7%)
  other arithmetic  3.23 us (2%)
  between operations  2.92 us (2%)
    all_to_all x1, blocking collectives, sent_to_all(): return lax.all_to_all(copies, axis, split_axis=0, concat_axis=0, tiled=True)  36.4 us
    all_to_all x1, blocking collectives, turned_gather(): pieces = lax.all_to_all(pieces, axis, split_axis=0, concat_axis=0)  33.9 us
    psum x4, blocking collectives, by_axis(): array = lax.psum(array, axis)  33.1 us
    all_gather x1, blocking collectives, in_one_piece_2(): filled = lax.all_gather(both, axis, axis=dim, tiled=True)  21.7 us
    all_to_all x1, blocking collectives, sent_and_summed(): lax.all_to_all(blocks, axis, split_axis=0, concat_axis=0, tiled=True)  15.3 us
    dot_general x2, matrix products, shards(): jnp.dot(pairs[number][0], wholes[number], preferred_element_type=jnp.floa...  8.31 us
    unnamed x28, local copies, waits for them, and re-layouts  4.87 us
    all_to_all x1, local copies, waits for them, and re-layouts, turned_gather(): pieces = lax.all_to_all(pieces, axis, split_axis=0, concat_axis=0)  4.38 us

profile of v1, /device:TPU:0, one launch (start us, length us, event | category | flops | bytes accessed | tf_op | source)
XLA Modules:
  0.0 172.4 jit_solution(16301961745324588500)
XLA Ops:
  0.7 1.0 pad_maximum_fusion.2
  1.9 36.4 %all_to_all.15 = bf16[16,128,512]{2,1,0:T(8,128)(2,1)S(1)} all-to-all(bf16[16,128,512]{2,1,0:T(8,128)(2,1)S(1)} %broadcast_in_dim.3), channel_id=1, replica_groups=mesh['fs_0'=4,'fs_1'=4,'tp_0'=4,'tp_1'=2] {'fs_0','fs_1'}, dimensions={0} | all-to-all | bytes 4194304 | tf_op jit(solution)/shard_map/all_to_all | solution.py:23
  38.3 5.9 %fusion.10 = (bf16[2048,256]{0,1:T(8,128)(2,1)S(1)}, f32[2048,256]{0,1:T(8,128)S(1)}) fusion(bf16[2048,2048]{1,0:T(8,128)(2,1)} %param.15, bf16[2048,512]{1,0:T(8,128)(2,1)S(1)} %bitcast.25), kind=kOutput, calls=%fused_computation.33 | convolution fusion | flops 2148007936 | bytes 12582912 | tf_op jit(solution)/shard_map/dot_general | solution.py:125
  44.3 2.4 %fusion.11 = (bf16[2048,256]{0,1:T(8,128)(2,1)S(1)}, f32[2048,256]{0,1:T(8,128)S(1)}) fusion(bf16[2048,2048]{1,0:T(8,128)(2,1)S(1)} %bitcast.28, bf16[2048,512]{1,0:T(8,128)(2,1)S(1)} %bitcast.26), kind=kOutput, calls=%fused_computation.34 | convolution fusion | flops 2148007936 | bytes 12582912 | tf_op jit(solution)/shard_map/dot_general | solution.py:125
  46.7 0.5 fusion.13
  47.2 0.5 convolution_add_fusion
  47.8 0.8 copy-done.1
  48.5 0.5 fusion.12
  49.1 0.6 convolution_add_fusion.1
  50.1 15.3 %all_to_all.16 = f32[16,16,640]{2,1,0:T(8,128)S(1)} all-to-all(f32[16,16,640]{2,1,0:T(8,128)S(1)} %bitcast.24), channel_id=1, replica_groups=mesh['fs_0'=4,'fs_1'=4,'tp_0'=4,'tp_1'=2] {'fs_0','fs_1'}, dimensions={0} | all-to-all | bytes 1310720 | tf_op jit(solution)/shard_map/all_to_all | solution.py:47
  65.4 0.7 multiply_reduce_fusion
  67.4 9.1 %psum.28 = f32[]{:T(128)} all-reduce(f32[]{:T(128)S(6)} %add.42), channel_id=1, replica_groups=mesh['fs_0'=4,'fs_1'=4,'tp_0'=4,'tp_1'=2] {'fs_0'}, use_global_device_ids=true, to_apply=%region_3.0 | all-reduce | flops 1 | bytes 8 | tf_op jit(solution)/shard_map/psum | solution.py:62
  76.4 9.5 %psum.29 = f32[]{:T(128)} all-reduce(f32[]{:T(128)} %psum.28), channel_id=1, replica_groups=mesh['fs_0'=4,'fs_1'=4,'tp_0'=4,'tp_1'=2] {'fs_1'}, use_global_device_ids=true, to_apply=%region_4.0 | all-reduce | flops 1 | bytes 8 | tf_op jit(solution)/shard_map/psum | solution.py:62
  86.0 11.3 %psum.30 = f32[]{:T(128)} all-reduce(f32[]{:T(128)} %psum.29), channel_id=1, replica_groups=mesh['fs_0'=4,'fs_1'=4,'tp_0'=4,'tp_1'=2] {'tp_0'}, use_global_device_ids=true, to_apply=%region_5.0 | all-reduce | flops 1 | bytes 8 | tf_op jit(solution)/shard_map/psum | solution.py:62
  97.3 3.1 %psum.31 = f32[]{:T(128)} all-reduce(f32[]{:T(128)} %psum.30), channel_id=1, replica_groups=mesh['fs_0'=4,'fs_1'=4,'tp_0'=4,'tp_1'=2] {'tp_1'}, use_global_device_ids=true, to_apply=%region_6.0 | all-reduce | flops 1 | bytes 8 | tf_op jit(solution)/shard_map/psum | solution.py:62
  101.1 0.7 divide_convert_fusion.1
  101.9 21.7 %all_gather.3 = bf16[256,640]{1,0:T(8,128)(2,1)S(1)} all-gather(bf16[16,640]{1,0:T(8,128)(2,1)S(1)} %pad_maximum_fusion.3), channel_id=1, replica_groups=mesh['fs_0'=4,'fs_1'=4,'tp_0'=4,'tp_1'=2] {'fs_0','fs_1'}, dimensions={0}, use_global_device_ids=true | all-gather | bytes 348160 | tf_op jit(solution)/shard_map/all_gather | solution.py:69
  123.9 1.0 fusion.7
  124.9 0.7 convert_bitcast_fusion
  126.1 33.9 %all_to_all.17 = bf16[16,128,640]{1,2,0:T(8,128)(2,1)} all-to-all(bf16[16,128,640]{1,2,0:T(8,128)(2,1)S(1)} %stack.2), channel_id=1, replica_groups=mesh['fs_0'=4,'fs_1'=4,'tp_0'=4,'tp_1'=2] {'fs_0','fs_1'}, dimensions={0} | all-to-all | bytes 5242880 | tf_op jit(solution)/shard_map/all_to_all | solution.py:79
  160.1 4.4 %copy.25 = bf16[16,128,640]{2,1,0:T(8,128)(2,1)} copy(bf16[16,128,640]{1,2,0:T(8,128)(2,1)} %all_to_all.17) | data formatting | bytes 5242880 | tf_op jit(solution)/shard_map/all_to_all | solution.py:79
  164.5 3.9 %slice_bitcast_fusion = (bf16[320,2048]{0,1:T(8,128)(2,1)}, bf16[2048,320]{1,0:T(8,128)(2,1)S(1)}) fusion(bf16[2048,640]{1,0:T(8,128)(2,1)} %bitcast.23), kind=kLoop, calls=%fused_computation.4 | loop fusion | bytes 5242880 | tf_op jit(solution)/shard_map/transpose | solution.py:84
  168.4 2.5 %copy.27 = bf16[320,2048]{1,0:T(8,128)(2,1)} copy(bf16[320,2048]{0,1:T(8,128)(2,1)} %get-tuple-element.32) | data formatting | bytes 2621440
  170.9 1.5 copy.26
  (34 shorter events, 1.5 us)
Async XLA Ops:
  0.6 46.0 %copy-start = (bf16[2048,320]{0,1:T(8,128)(2,1)S(1)}, bf16[2048,320]{0,1:T(8,128)(2,1)}, u32[]{:S(2)}) copy-start(bf16[2048,320]{0,1:T(8,128)(2,1)} %param.14) | copy-start | bytes 3932164
  1.8 42.4 %slice-start = ((s8[8388608]{0:T(1024)(128)(4,1)}), s8[4194304]{0:T(1024)(128)(4,1)S(1)}, s32[]{:S(2)}) async-start(s8[8388608]{0:T(1024)(128)(4,1)} %bitcast.27), calls=%async_computation.3 | async-start | bytes 8388608
  38.3 5.9 %slice-start.1 = ((s8[8388608]{0:T(1024)(128)(4,1)}), s8[4194304]{0:T(1024)(128)(4,1)S(1)}, s32[]{:S(2)}) async-start(s8[8388608]{0:T(1024)(128)(4,1)} %bitcast.27), calls=%async_computation.4 | async-start | bytes 8388608
  47.2 1.3 copy-start.1
  49.7 51.4 %copy-start.7 = (f32[16,320]{1,0:T(8,128)S(1)}, f32[16,320]{1,0:T(8,128)}, u32[]{:S(2)}) copy-start(f32[16,320]{1,0:T(8,128)} %param.21) | copy-start | bytes 61444
  49.7 51.4 %copy-start.8 = (f32[16,320]{1,0:T(8,128)S(1)}, f32[16,320]{1,0:T(8,128)}, u32[]{:S(2)}) copy-start(f32[16,320]{1,0:T(8,128)} %param.20) | copy-start | bytes 61444
  49.7 51.4 %copy-start.9 = (f32[16,320]{1,0:T(8,128)S(1)}, f32[16,320]{1,0:T(8,128)}, u32[]{:S(2)}) copy-start(f32[16,320]{1,0:T(8,128)} %param.23) | copy-start | bytes 61444
  49.7 51.4 %copy-start.10 = (f32[16,320]{1,0:T(8,128)S(1)}, f32[16,320]{1,0:T(8,128)}, u32[]{:S(2)}) copy-start(f32[16,320]{1,0:T(8,128)} %param.22) | copy-start | bytes 61444
  49.8 73.8 %copy-start.4 = (bf16[128,256]{1,0:T(8,128)(2,1)S(1)}, bf16[128,256]{1,0:T(8,128)(2,1)}, u32[]{:S(2)}) copy-start(bf16[128,256]{1,0:T(8,128)(2,1)} %param.17) | copy-start | bytes 196612
  49.8 74.1 %copy-start.3 = (bf16[128,256]{1,0:T(8,128)(2,1)S(1)}, bf16[128,256]{1,0:T(8,128)(2,1)}, u32[]{:S(2)}) copy-start(bf16[128,256]{1,0:T(8,128)(2,1)} %param.16) | copy-start | bytes 196612
  49.8 74.1 %copy-start.5 = (f32[128,320]{0,1:T(8,128)S(1)}, f32[128,320]{0,1:T(8,128)}, u32[]{:S(2)}) copy-start(f32[128,320]{0,1:T(8,128)} %param.18) | copy-start | bytes 491524
  50.0 74.9 %copy-start.6 = (f32[320,128]{1,0:T(8,128)S(1)}, f32[320,128]{1,0:T(8,128)}, u32[]{:S(2)}) copy-start(f32[320,128]{1,0:T(8,128)} %param.19) | copy-start | bytes 491524
  123.9 2.2 %copy-start.2 = (f32[320,128]{1,0:T(8,128)}, f32[320,128]{1,0:T(8,128)S(1)}, u32[]{:S(2)}) copy-start(f32[320,128]{1,0:T(8,128)S(1)} %fusion.2) | copy-start | bytes 491524
